TPU v7x, 32 devices: a whole 2x2x4 slice. The times are simulated.
32 devices in a mesh: sp: 8 (over z, x), tp: 4 (over y, core).
Axes of the slice: x: 2, y: 2, z: 4, core: 2. Of those that a mesh axis runs over, the one named last changes fastest.
Arguments:
- queries: bfloat16 [1024, 2048], P('sp', 'tp'), may hold values from -18 to 90
- projected_key_rows: bfloat16 [1024, 1024], P('sp', 'tp'), may hold values from -18 to 90
- projected_value_rows: bfloat16 [1024, 1024], P('sp', 'tp'), may hold values from -6 to 6
- query_gain: float32 [64], replicated, may hold values from 1 to 6
- key_norm_gain: float32 [64], replicated, may hold values from 1 to 6
- residual: bfloat16 [1024, 2048], P('sp', 'tp'), may hold values from -54 to 54
- out_weight: bfloat16 [2048, 2048], P('tp'), may hold values from -1 to 1
- norm_gain: float32 [2048], P('tp'), may hold values from 0.28 to 4.68
- expert_ids: int32 [1024, 2], P('sp'), may hold values from 0 to 7, as said below
- route_weights: float32 [1024, 2], P('sp'), may hold values from 0.2 to 1
- gate_weight: bfloat16 [8, 2048, 4096], P('sp', None, 'tp'), may hold values from -0.125 to 0.125
- up_weight: bfloat16 [8, 2048, 4096], P('sp', None, 'tp'), may hold values from -0.125 to 0.125
- down_weight: bfloat16 [8, 4096, 2048], P('sp', 'tp'), may hold values from -0.25 to 0.25
- final_gain: float32 [2048], P('tp'), may hold values from 0.1 to 1.9
Outputs:
- layer_out: bfloat16 [1024, 2048], P('sp', 'tp')
Inputs may be any that keep to these rules, and one draw needn't show every extreme that they name: `expert_ids`: each row names two different experts of one group, the group of expert e being e // 4. In every aligned block of 128 rows each group is named by the same number of rows, no expert is named by more than 64 rows, one expert of every group is named by exactly 64 rows, and one expert is named by 64 rows of every block.
All inputs are finite; a program needn't handle non-finite values.
Results may differ from a plain program's by a relative error of at most 0.019.
The roundings to bfloat16 on the way count: a program that leaves them out, or rounds other values in their place, can miss the bound.
Values may be sent and summed in bfloat16 or wider, within the bound.
A program may use at most 64 MiB of HBM per device.

v0:
```python
from functools import reduce
import jax
import jax.numpy as jnp
from jax import lax
from jax.sharding import PartitionSpec as P

D = 2048
HEAD_DIM = 64
GRID_W = 64
TOPK = 2
theta_base = 10000.0
norm_epsilon = 1e-06
residual_scale = 8.0**0.25
far_below = -1e30


def rope_line(halves, angles):
    pair_count = angles.shape[-1]
    first_half = halves[..., :pair_count]
    second_half = halves[..., pair_count:]
    cosine = jnp.cos(angles)[:, None, :]
    sine_part = jnp.sin(angles)[:, None, :]
    return jnp.concatenate(
        [
            first_half * cosine - second_half * sine_part,
            first_half * sine_part + second_half * cosine,
        ],
        -1,
    )


def rotary_over_grid(rows_by_head, token_positions):
    head_size = rows_by_head.shape[-1]
    frequency = theta_base ** (
        -jnp.arange(0, head_size // 2, 2, dtype=jnp.float32) / (head_size // 2)
    )
    grid_row = (token_positions // GRID_W).astype(jnp.float32)
    grid_col = (token_positions % GRID_W).astype(jnp.float32)
    row_part = rope_line(
        rows_by_head[..., : head_size // 2], grid_row[:, None] * frequency[None, :]
    )
    col_part = rope_line(
        rows_by_head[..., head_size // 2 :], grid_col[:, None] * frequency[None, :]
    )
    return jnp.concatenate([row_part, col_part], -1)


def normalize_heads(token_rows, gain_row, head_count):
    shaped = token_rows.astype(jnp.float32).reshape(token_rows.shape[0], head_count, -1)
    scaled = shaped * lax.rsqrt(jnp.mean(shaped * shaped, -1, keepdims=True) + norm_epsilon)
    return scaled * gain_row[None, None, :]


def norm_features(feature_rows, gain_row, feature_total):
    row_sums = jnp.sum(feature_rows, 0)
    squares = jnp.sum(feature_rows * feature_rows, 0)
    row_sums, squares = lax.psum((row_sums, squares), "tp")
    center = row_sums / feature_total
    spread = squares / feature_total - center * center
    return (
        (feature_rows - center[None, :])
        * lax.rsqrt(spread + norm_epsilon)[None, :]
        * gain_row[:, None]
    )


def per_device(
    queries,
    projected_key_rows,
    projected_value_rows,
    query_gain,
    key_norm_gain,
    residual,
    out_weight,
    norm_gain,
    expert_ids,
    route_weights,
    gate_weight,
    up_weight,
    down_weight,
    final_gain,
):
    token_count = queries.shape[0]
    query_heads = queries.shape[1] // HEAD_DIM
    key_heads = projected_key_rows.shape[1] // HEAD_DIM
    queries_per_group = query_heads // key_heads
    token_positions = lax.axis_index("sp") * token_count + jnp.arange(token_count, dtype=jnp.int32)
    queries_after_rotation = rotary_over_grid(
        normalize_heads(queries, query_gain, query_heads), token_positions
    ).astype(jnp.bfloat16)
    keys_after_rotation = rotary_over_grid(
        normalize_heads(projected_key_rows, key_norm_gain, key_heads), token_positions
    ).astype(jnp.bfloat16)
    packed = jnp.concatenate(
        [keys_after_rotation, projected_value_rows.reshape(token_count, key_heads, HEAD_DIM)], -1
    ).reshape(token_count, key_heads * 2 * HEAD_DIM)
    grouped_query_heads = (
        queries_after_rotation.reshape(token_count, key_heads, queries_per_group, HEAD_DIM)
        .transpose(1, 2, 0, 3)
        .reshape(key_heads, queries_per_group * token_count, HEAD_DIM)
    )
    score_scale = HEAD_DIM ** (-0.5)
    query_total = queries_per_group * token_count
    section = lax.all_gather(packed, "sp", axis=0, tiled=True)
    running_max = jnp.full((key_heads, query_total), far_below, jnp.float32)
    opened = section.reshape(section.shape[0], key_heads, 2 * HEAD_DIM)
    scores = (
        jnp.einsum(
            "hqd,khd->hqk",
            grouped_query_heads,
            opened[:, :, :HEAD_DIM],
            preferred_element_type=jnp.float32,
        )
        * score_scale
    )
    new_peak = jnp.maximum(running_max, jnp.max(scores, -1))
    weights = jnp.exp(scores - new_peak[:, :, None])
    running_sum = jnp.sum(weights, -1)
    running_out = jnp.einsum(
        "hqk,khd->hqd",
        weights.astype(jnp.bfloat16),
        opened[:, :, HEAD_DIM:],
        preferred_element_type=jnp.float32,
    )
    running_max, running_sum, running_out = (new_peak, running_sum, running_out)
    attended = (running_out / running_sum[:, :, None]).astype(jnp.bfloat16)
    attended = (
        attended.reshape(key_heads, queries_per_group, token_count, HEAD_DIM)
        .transpose(2, 0, 1, 3)
        .reshape(token_count, query_heads * HEAD_DIM)
    )
    local_width = residual.shape[1]
    columns = out_weight
    mixed_rows = lax.psum_scatter(
        lax.dot_general(
            columns, attended, (((0,), (1,)), ((), ())), preferred_element_type=jnp.float32
        ).astype(jnp.bfloat16),
        "tp",
        scatter_dimension=0,
        tiled=True,
    ).astype(jnp.float32)
    pre_norm = residual_scale * residual.astype(jnp.float32).T + mixed_rows
    normed = norm_features(pre_norm, norm_gain, D).astype(jnp.bfloat16)
    expert_count = lax.axis_size("sp")
    capacity = 4 * token_count // expert_count
    row_total = expert_count * capacity
    flat_ids = expert_ids.reshape(-1)
    marked = (flat_ids[:, None] == jnp.arange(expert_count, dtype=jnp.int32)[None, :]).astype(
        jnp.int32
    )
    earlier = jnp.cumsum(marked, 0) - marked
    places = (flat_ids * capacity + jnp.sum(earlier * marked, 1)).reshape(token_count, TOPK)
    lane_index = jnp.arange(row_total, dtype=jnp.int32)
    selectors = [
        (places[:, route_rank : route_rank + 1] == lane_index[None, :]).astype(jnp.bfloat16)
        for route_rank in range(TOPK)
    ]
    dispatch = reduce(jnp.add, selectors)
    gate_local = gate_weight[0]
    up_local = up_weight[0]
    down_local = down_weight[0]
    outgoing = lax.dot_general(
        dispatch, normed, (((0,), (1,)), ((), ())), preferred_element_type=jnp.float32
    ).astype(jnp.bfloat16)
    arrived = lax.all_to_all(
        outgoing.reshape(expert_count, capacity, local_width),
        "sp",
        split_axis=0,
        concat_axis=0,
        tiled=True,
    ).reshape(row_total, local_width)
    section = lax.all_gather(arrived, "tp", axis=1, tiled=True)
    gate_sum = jnp.dot(section, gate_local, preferred_element_type=jnp.float32)
    up_sum = jnp.dot(section, up_local, preferred_element_type=jnp.float32)
    hidden = (jax.nn.silu(gate_sum) * up_sum).astype(jnp.bfloat16)
    columns = down_local
    expert_out = lax.psum_scatter(
        lax.dot_general(
            columns, hidden, (((0,), (1,)), ((), ())), preferred_element_type=jnp.float32
        ).astype(jnp.bfloat16),
        "tp",
        scatter_dimension=0,
        tiled=True,
    )
    returned = lax.all_to_all(
        expert_out.reshape(local_width, expert_count, capacity),
        "sp",
        split_axis=1,
        concat_axis=1,
        tiled=True,
    ).reshape(local_width, row_total)
    combined = jnp.zeros((local_width, token_count), jnp.float32)
    for route_rank in range(TOPK):
        chosen = lax.dot_general(
            returned,
            selectors[route_rank],
            (((1,), (1,)), ((), ())),
            preferred_element_type=jnp.float32,
        )
        combined = combined + chosen * route_weights[:, route_rank][None, :]
    second_sum = residual_scale * normed.astype(jnp.float32) + combined
    return norm_features(second_sum, final_gain, D).T.astype(jnp.bfloat16)


def solution(mesh):
    in_specs = (
        P("sp", "tp"),
        P("sp", "tp"),
        P("sp", "tp"),
        P(),
        P(),
        P("sp", "tp"),
        P("tp", None),
        P("tp"),
        P("sp", None),
        P("sp", None),
        P("sp", None, "tp"),
        P("sp", None, "tp"),
        P("sp", "tp", None),
        P("tp"),
    )
    out_specs = P("sp", "tp")
    return jax.shard_map(
        per_device, mesh=mesh, in_specs=in_specs, out_specs=out_specs, check_vma=False
    )
```

profile of v0, /device:TPU:0, one launch (start us, length us, event | category | flops | bytes accessed | tf_op | source)
XLA Modules:
  0.0 209.7 jit_solution(3007069951881743205)
XLA Ops:
  6.5 0.0 copy-start
  6.6 1.1 copy.42
  7.7 0.7 fusion.43
  8.5 0.1 multiply_cosine_fusion
  8.7 1.0 copy.43
  9.7 0.0 copy-start.2
  9.7 0.6 copy-done.2
  10.3 0.0 all-gather.3.cloned.1.call-update
  10.3 0.0 reduce-scatter.3.cloned.1.call-start
  10.4 1.0 copy.40
  11.5 0.7 fusion.38
  12.3 40.3 %all-gather.3.cloned.1.call-done = bf16[1024,512]{0,1:T(8,128)(2,1)} async-done(((bf16[128,512]{0,1:T(8,128)(2,1)}), bf16[1024,512]{0,1:T(8,128)(2,1)}) %all-gather.3.cloned.1.call-update) | async-done | bytes 1048592 | tf_op jit(solution)/shard_map/all_gather | solution.py:104
  52.6 2.0 multiply_reduce_fusion
  54.6 0.9 fusion.6
  55.5 0.0 copy-start.5
  55.5 0.0 copy-start.3
  55.5 0.0 copy-start.8
  55.5 0.9 fusion.29
  56.5 1.3 fusion.14
  57.8 0.0 reduce-scatter.3.cloned.1.call-update
  57.8 0.0 all-gather.5.cloned.1.call-start
  57.9 0.1 copy.45
  58.0 0.1 eq.62
  58.1 0.1 eq.58
  58.3 0.6 reduce-window.6
  58.9 0.2 slice_reduce_fusion
  59.1 0.1 fusion.59
  59.2 0.1 reduce_sum.80
  59.4 0.1 copy.47
  59.5 19.2 %reduce-scatter.3.cloned.1.call-done = bf16[512,128]{0,1:T(8,128)(2,1)} async-done(((bf16[2048,128]{0,1:T(8,128)(2,1)}), bf16[512,128]{0,1:T(8,128)(2,1)}) %reduce-scatter.3.cloned.1.call-update) | async-done | bytes 131088 | tf_op jit(solution)/shard_map/reduce_scatter | solution.py:134
  78.7 1.0 fusion.41
  79.7 5.8 %all-reduce.1 = (f32[128]{0:T(128)S(1)}, f32[128]{0:T(128)S(1)}) all-reduce(f32[128]{0:T(128)S(1)} %get-tuple-element.8, f32[128]{0:T(128)S(1)} %get-tuple-element.7), channel_id=1, replica_groups=mesh['sp'=8,'tp'=4] {'tp'}, use_global_device_ids=true, to_apply=%region_8.9 | all-reduce | flops 256 | bytes 2048 | tf_op jit(solution)/shard_map/psum | solution.py:57
  85.5 1.3 convolution_convert_fusion.1
  86.8 19.8 %all_to_all.10 = bf16[8,64,512]{2,1,0:T(8,128)(2,1)} all-to-all(bf16[8,64,512]{2,1,0:T(8,128)(2,1)S(1)} %bitcast.97), channel_id=1, replica_groups=mesh['sp'=8,'tp'=4] {'sp'}, dimensions={0} | all-to-all | bytes 1048576 | tf_op jit(solution)/shard_map/all_to_all | solution.py:165
  106.6 0.0 all-gather.5.cloned.1.call-update
  106.7 0.0 reduce-scatter.5.cloned.1.call-start
  106.7 20.8 %all-gather.5.cloned.1.call-done = bf16[512,2048]{1,0:T(8,128)(2,1)} async-done(((bf16[512,512]{1,0:T(8,128)(2,1)}), bf16[512,2048]{1,0:T(8,128)(2,1)}) %all-gather.5.cloned.1.call-update) | async-done | bytes 2097168 | tf_op jit(solution)/shard_map/all_gather | solution.py:172
  127.5 6.5 %fusion.4 = f32[512,1024]{1,0:T(8,128)} fusion(bf16[512,2048]{1,0:T(8,128)(2,1)} %all-gather.5.cloned.1.call-done, bf16[1,2048,1024]{2,1,0:T(8,128)(2,1)} %param.24), kind=kOutput, calls=%fused_computation.4 | convolution fusion | flops 2147483648 | bytes 8388608 | tf_op jit(solution)/shard_map/dot_general | solution.py:173
  134.0 10.6 %fusion.11 = bf16[2048,512]{0,1:T(8,128)(2,1)} fusion(bf16[1,1024,2048]{2,1,0:T(8,128)(2,1)} %param.26, f32[512,1024]{1,0:T(8,128)} %fusion.4, bf16[512,2048]{1,0:T(8,128)(2,1)} %all-gather.5.cloned.1.call-done, bf16[1,2048,1024]{2,1,0:T(8,128)(2,1)} %param.25), kind=kOutput, calls=%fused_computation.11 | convolution fusion | flops 4299161600 | bytes 14680064 | tf_op jit(solution)/shard_map/dot_general | solution.py:178
  144.6 0.0 reduce-scatter.5.cloned.1.call-update
  144.6 31.3 %reduce-scatter.5.cloned.1.call-done = bf16[512,512]{0,1:T(8,128)(2,1)} async-done(((bf16[2048,512]{0,1:T(8,128)(2,1)}), bf16[512,512]{0,1:T(8,128)(2,1)}) %reduce-scatter.5.cloned.1.call-update) | async-done | bytes 524304 | tf_op jit(solution)/shard_map/reduce_scatter | solution.py:177
  175.9 5.5 %all-to-all-start.1 = ((bf16[512,8,64]{0,2,1:T(8,128)(2,1)}), bf16[512,8,64]{0,2,1:T(8,128)(2,1)S(1)}, u32[]{:S(2)}, u32[]{:S(2)}) async-start(bf16[512,8,64]{0,2,1:T(8,128)(2,1)} %bitcast.96), calls=%async_computation.3 | async-start | bytes 1048576 | tf_op jit(solution)/shard_map/all_to_all | solution.py:185
  181.5 14.3 %all-to-all-done.1 = bf16[512,8,64]{0,2,1:T(8,128)(2,1)S(1)} async-done(((bf16[512,8,64]{0,2,1:T(8,128)(2,1)}), bf16[512,8,64]{0,2,1:T(8,128)(2,1)S(1)}, u32[]{:S(2)}, u32[]{:S(2)}) %all-to-all-start.1) | async-done | bytes 524320 | tf_op jit(solution)/shard_map/all_to_all | solution.py:185
  195.8 0.3 convolution_multiply_fusion.1
  196.1 0.0 copy-done.4
  196.1 0.4 fusion.65
  196.5 5.9 %all-reduce = (f32[128]{0:T(128)S(1)}, f32[128]{0:T(128)S(1)}) all-reduce(f32[128]{0:T(128)S(1)} %get-tuple-element.6, f32[128]{0:T(128)S(1)} %get-tuple-element.5), channel_id=1, replica_groups=mesh['sp'=8,'tp'=4] {'tp'}, use_global_device_ids=true, to_apply=%region_16.17 | all-reduce | flops 256 | bytes 2048 | tf_op jit(solution)/shard_map/psum | solution.py:57
  202.4 0.8 fusion.47
  (34 shorter events, 0.4 us)
Async XLA Ops:
  6.5 50.0 %copy-start = (bf16[512,2048]{1,0:T(8,128)(2,1)S(1)}, bf16[512,2048]{1,0:T(8,128)(2,1)}, u32[]{:S(2)}) copy-start(bf16[512,2048]{1,0:T(8,128)(2,1)} %param.20) | copy-start | bytes 6291460
  6.5 46.1 %all-gather.3.cloned.1.call-start = ((), (), s32[]{:S(2)}) async-start(), calls=%async_computation.4 | async-start | bytes 1179648 | tf_op jit(solution)/shard_map/all_gather | solution.py:104
  9.7 0.7 copy-start.2
  10.3 68.3 %reduce-scatter.3.cloned.1.call-start = ((), (), s32[]{:S(2)}) async-start(), calls=%async_computation.5 | async-start | bytes 655360 | tf_op jit(solution)/shard_map/reduce_scatter | solution.py:134
  52.6 2.9 %copy-start.1 = (bf16[1024,512]{0,1:T(8,128)(2,1)S(1)}, bf16[1024,512]{0,1:T(8,128)(2,1)}, u32[]{:S(2)}) copy-start(bf16[1024,512]{0,1:T(8,128)(2,1)} %all-gather.3.cloned.1.call-done) | copy-start | bytes 3145732
  55.5 2.4 %copy-start.5 = (s32[128,2]{0,1:T(2,128)S(1)}, s32[128,2]{0,1:T(2,128)}, u32[]{:S(2)}) copy-start(s32[128,2]{0,1:T(2,128)} %param.22) | copy-start | bytes 3076
  55.5 23.2 %copy-start.3 = (bf16[128,512]{1,0:T(8,128)(2,1)S(1)}, bf16[128,512]{1,0:T(8,128)(2,1)}, u32[]{:S(2)}) copy-start(bf16[128,512]{1,0:T(8,128)(2,1)} %param.19) | copy-start | bytes 393220
  55.5 30.0 %copy-start.8 = (f32[512]{0:T(512)S(1)}, f32[512]{0:T(512)}, u32[]{:S(2)}) copy-start(f32[512]{0:T(512)} %param.21) | copy-start | bytes 6148
  57.8 69.7 %all-gather.5.cloned.1.call-start = ((), (), s32[]{:S(2)}) async-start(), calls=%async_computation.6 | async-start | bytes 2621440 | tf_op jit(solution)/shard_map/all_gather | solution.py:172
  106.7 69.3 %reduce-scatter.5.cloned.1.call-start = ((), (), s32[]{:S(2)}) async-start(), calls=%async_computation.7 | async-start | bytes 2621440 | tf_op jit(solution)/shard_map/reduce_scatter | solution.py:177
  134.0 47.4 %copy-start.7 = (f32[128,2]{0,1:T(2,128)S(1)}, f32[128,2]{0,1:T(2,128)}, u32[]{:S(2)}) copy-start(f32[128,2]{0,1:T(2,128)} %param.23) | copy-start | bytes 3076
  134.0 62.0 %copy-start.4 = (bf16[512,128]{0,1:T(8,128)(2,1)S(1)}, bf16[512,128]{0,1:T(8,128)(2,1)}, u32[]{:S(2)}) copy-start(bf16[512,128]{0,1:T(8,128)(2,1)} %reduce-scatter.3.cloned.1.call-done) | copy-start | bytes 393220
  144.6 57.8 %copy-start.6 = (f32[512]{0:T(512)S(1)}, f32[512]{0:T(512)}, u32[]{:S(2)}) copy-start(f32[512]{0:T(512)} %param.27) | copy-start | bytes 6148
  175.9 19.8 %all-to-all-start.1 = ((bf16[512,8,64]{0,2,1:T(8,128)(2,1)}), bf16[512,8,64]{0,2,1:T(8,128)(2,1)S(1)}, u32[]{:S(2)}, u32[]{:S(2)}) async-start(bf16[512,8,64]{0,2,1:T(8,128)(2,1)} %bitcast.96), calls=%async_computation.3 | async-start | bytes 1048576 | tf_op jit(solution)/shard_map/all_to_all | solution.py:185
Sparse Core Ops, SparseCore 0:
  10.5 42.1 all-gather.2
  57.9 20.6 reduce-scatter.2
  106.8 20.7 all-gather.4
  144.7 31.1 reduce-scatter.4
where the time goes:
time: 210 us
  waiting for transfers between devices  126 us (60%)
  blocking collectives  31.5 us (15%)
  matrix products  23.2 us (11%)
  between operations  13.4 us (6%)
  starting transfers between devices  5.64 us (3%)
  other arithmetic  5.31 us (3%)
  local copies, waits for them, and re-layouts  4.61 us (2%)
    all_gather x1, waiting for transfers between devices, per_device(): section = lax.all_gather(packed, 'sp', axis=0, tiled=True)  40.3 us
    reduce_scatter x1, waiting for transfers between devices, per_device(): lax.psum_scatter(lax.dot_general(columns, hidden, (((0,), (1,)), ((), ())...  31.3 us
    all_gather x1, waiting for transfers between devices, per_device(): section = lax.all_gather(arrived, 'tp', axis=1, tiled=True)  20.8 us
    all_to_all x1, blocking collectives, per_device(): lax.all_to_all(outgoing.reshape(expert_count, capacity, local_width), 'sp...  19.8 us
    reduce_scatter x1, waiting for transfers between devices, per_device(): lax.psum_scatter(lax.dot_general(columns, attended, (((0,), (1,)), ((), (...  19.2 us
    all_to_all x1, waiting for transfers between devices, per_device(): lax.all_to_all(expert_out.reshape(local_width, expert_count, capacity), '...  14.3 us
    psum x2, blocking collectives, norm_features(): row_sums, squares = lax.psum((row_sums, squares), 'tp')  11.7 us
    dot_general x1, matrix products, per_device(): lax.dot_general(columns, hidden, (((0,), (1,)), ((), ())), preferred_elem...  10.6 us
  transfers between devices with their start and end apart: 5, of which 5 were waited for; matrix products, arithmetic and copies ran while one was open for 2% of the time, Pallas kernels for 0%

commit v1 on v0

--- a/solution.py
+++ b/solution.py
@@ -169,7 +169,12 @@
         concat_axis=0,
         tiled=True,
     ).reshape(row_total, local_width)
-    section = lax.all_gather(arrived, "tp", axis=1, tiled=True)
+    ring = [arrived]
+    for hop in range(3):
+        ring.append(lax.ppermute(ring[-1], "tp", [(dev, (dev + 1) % 4) for dev in range(4)]))
+    section = jnp.roll(
+        jnp.concatenate(ring[::-1], axis=1), (lax.axis_index("tp") + 1) * ring[0].shape[1], axis=1
+    )
     gate_sum = jnp.dot(section, gate_local, preferred_element_type=jnp.float32)
     up_sum = jnp.dot(section, up_local, preferred_element_type=jnp.float32)
     hidden = (jax.nn.silu(gate_sum) * up_sum).astype(jnp.bfloat16)

time: 210 us -> 218 us (1.038)
  local copies, waits for them, and re-layouts: 4.61 us -> 11.3 us
  waiting for transfers between devices: 126 us -> 130 us
  matrix products: 23.2 us -> 20.5 us
    ppermute x0 -> x3, waiting for transfers between devices: none -> 26.2 us  [per_device(): lax.ppermute(ring[-1], 'tp', [(dev, (dev + 1) % 4) for dev in range(4)])]
    all_gather x1 -> x0, waiting for transfers between devices: 20.8 us -> none  [per_device(): section = lax.all_gather(arrived, 'tp', axis=1, tiled=True)]
    unnamed x22 -> x33, local copies, waits for them, and re-layouts: 3.87 us -> 10.4 us
    dot_general x1, matrix products: 6.48 us -> 3.71 us  [per_device(): gate_sum = jnp.dot(section, gate_local, preferred_element_type=jnp.float32)]
  transfers between devices with their start and end apart: 5 -> 7, of which waited for: 5 -> 7; matrix products, arithmetic and copies ran while one was open for 2% -> 2% of each run, Pallas kernels for 0% -> 0%
where the time goes in v1:
time: 218 us; the launch traced here: 217 us
  waiting for transfers between devices  130 us (60%)
  blocking collectives  31.4 us (14%)
  matrix products  20.5 us (9%)
  between operations  13.4 us (6%)
  local copies, waits for them, and re-layouts  11.3 us (5%)
  starting transfers between devices  5.61 us (3%)
  other arithmetic  5.31 us (2%)
    all_gather x1, waiting for transfers between devices, per_device(): section = lax.all_gather(packed, 'sp', axis=0, tiled=True)  40.3 us
    reduce_scatter x1, waiting for transfers between devices, per_device(): lax.psum_scatter(lax.dot_general(columns, hidden, (((0,), (1,)), ((), ())...  29.5 us
    ppermute x3, waiting for transfers between devices, per_device(): lax.ppermute(ring[-1], 'tp', [(dev, (dev + 1) % 4) for dev in range(4)])  26.2 us
    all_to_all x1, blocking collectives, per_device(): lax.all_to_all(outgoing.reshape(expert_count, capacity, local_width), 'sp...  19.7 us
    reduce_scatter x1, waiting for transfers between devices, per_device(): lax.psum_scatter(lax.dot_general(columns, attended, (((0,), (1,)), ((), (...  19.2 us
    all_to_all x1, waiting for transfers between devices, per_device(): lax.all_to_all(expert_out.reshape(local_width, expert_count, capacity), '...  14.3 us
    psum x2, blocking collectives, norm_features(): row_sums, squares = lax.psum((row_sums, squares), 'tp')  11.7 us
    dot_general x1, matrix products, per_device(): lax.dot_general(columns, hidden, (((0,), (1,)), ((), ())), preferred_elem...  10.6 us
  transfers between devices with their start and end apart: 7, of which 7 were waited for; matrix products, arithmetic and copies ran while one was open for 2% of the time, Pallas kernels for 0%

profile of v1, /device:TPU:0, one launch (start us, length us, event | category | flops | bytes accessed | tf_op | source)
XLA Modules:
  0.0 217.1 jit_solution(2969669056887955363)
XLA Ops:
  6.6 1.1 copy.42
  7.7 0.7 fusion.49
  8.5 0.1 multiply_cosine_fusion
  8.7 1.0 copy.43
  9.7 0.6 copy-done.2
  10.3 0.0 reduce-scatter.3.cloned.1.call-start
  10.4 1.0 copy.40
  11.5 0.7 fusion.44
  12.3 40.3 %all-gather.2.cloned.1.call-done = bf16[1024,512]{0,1:T(8,128)(2,1)} async-done(((bf16[128,512]{0,1:T(8,128)(2,1)}), bf16[1024,512]{0,1:T(8,128)(2,1)}) %all-gather.2.cloned.1.call-update) | async-done | bytes 1048592 | tf_op jit(solution)/shard_map/all_gather | solution.py:104
  52.6 2.0 multiply_reduce_fusion
  54.6 0.9 fusion.6
  55.5 0.9 fusion.33
  56.5 1.3 fusion.14
  57.8 0.0 reduce-scatter.5.cloned.1.call-start
  57.9 0.1 copy.45
  58.0 0.1 eq.65
  58.1 0.1 eq.61
  58.3 0.6 reduce-window.6
  58.9 0.2 slice_reduce_fusion
  59.1 0.1 fusion.61
  59.2 0.1 reduce_sum.80
  59.4 0.1 copy.47
  59.5 19.2 %reduce-scatter.3.cloned.1.call-done = bf16[512,128]{0,1:T(8,128)(2,1)} async-done(((bf16[2048,128]{0,1:T(8,128)(2,1)}), bf16[512,128]{0,1:T(8,128)(2,1)}) %reduce-scatter.3.cloned.1.call-update) | async-done | bytes 131088 | tf_op jit(solution)/shard_map/reduce_scatter | solution.py:134
  78.7 1.0 fusion.47
  79.7 5.8 %all-reduce.1 = (f32[128]{0:T(128)S(1)}, f32[128]{0:T(128)S(1)}) all-reduce(f32[128]{0:T(128)S(1)} %get-tuple-element.8, f32[128]{0:T(128)S(1)} %get-tuple-element.7), channel_id=1, replica_groups=mesh['sp'=8,'tp'=4] {'tp'}, use_global_device_ids=true, to_apply=%region_8.9 | all-reduce | flops 256 | bytes 2048 | tf_op jit(solution)/shard_map/psum | solution.py:57
  85.5 1.3 convolution_convert_fusion.1
  86.8 19.7 %all_to_all.10 = bf16[8,64,512]{2,1,0:T(8,128)(2,1)S(1)} all-to-all(bf16[8,64,512]{2,1,0:T(8,128)(2,1)S(1)} %bitcast.97), channel_id=1, replica_groups=mesh['sp'=8,'tp'=4] {'sp'}, dimensions={0} | all-to-all | bytes 1048576 | tf_op jit(solution)/shard_map/all_to_all | solution.py:165
  106.5 8.6 %collective-permute-done = bf16[512,512]{1,0:T(8,128)(2,1)S(1)} collective-permute-done((bf16[512,512]{1,0:T(8,128)(2,1)S(1)}, bf16[512,512]{1,0:T(8,128)(2,1)S(1)}, u32[]{:S(2)}, u32[]{:S(2)}) %collective-permute-start) | collective-permute-done | bytes 524320 | tf_op jit(solution)/shard_map/ppermute | solution.py:174
  115.2 8.7 %collective-permute-done.1 = bf16[512,512]{1,0:T(8,128)(2,1)} collective-permute-done((bf16[512,512]{1,0:T(8,128)(2,1)S(1)}, bf16[512,512]{1,0:T(8,128)(2,1)}, u32[]{:S(2)}, u32[]{:S(2)}) %collective-permute-start.1) | collective-permute-done | bytes 524320 | tf_op jit(solution)/shard_map/ppermute | solution.py:174
  123.9 8.9 %collective-permute-done.2 = bf16[512,512]{1,0:T(8,128)(2,1)} collective-permute-done((bf16[512,512]{1,0:T(8,128)(2,1)}, bf16[512,512]{1,0:T(8,128)(2,1)}, u32[]{:S(2)}, u32[]{:S(2)}) %collective-permute-start.2) | collective-permute-done | bytes 524320 | tf_op jit(solution)/shard_map/ppermute | solution.py:174
  132.8 1.1 constant_dynamic-update-slice_fusion.12
  133.9 1.1 constant_dynamic-update-slice_fusion.11
  135.0 0.1 constant_dynamic-update-slice_fusion.10
  135.1 0.1 constant_dynamic-update-slice_fusion.9
  135.2 1.1 constant_dynamic-update-slice_fusion.8
  136.3 1.1 constant_dynamic-update-slice_fusion.7
  137.4 0.1 constant_dynamic-update-slice_fusion.6
  137.5 0.1 constant_dynamic-update-slice_fusion.5
  137.6 1.9 copy-done.5
  139.5 3.7 %fusion.4 = f32[512,1024]{1,0:T(8,128)} fusion(bf16[1,2048,1024]{2,1,0:T(8,128)(2,1)S(1)} %copy-done.9, bf16[512,4096]{1,0:T(8,128)(2,1)S(1)} %constant_dynamic-update-slice_fusion.5, s32[]{:T(128)S(6)} %select_n.38), kind=kOutput, calls=%fused_computation.4 | convolution fusion | flops 2147483648 | bytes 8388612 | tf_op jit(solution)/shard_map/dot_general | solution.py:178
  143.2 10.6 %fusion.11 = bf16[2048,512]{0,1:T(8,128)(2,1)} fusion(bf16[1,1024,2048]{2,1,0:T(8,128)(2,1)} %param.26, f32[512,1024]{1,0:T(8,128)} %fusion.4, bf16[1,2048,1024]{2,1,0:T(8,128)(2,1)} %param.25, bf16[512,4096]{1,0:T(8,128)(2,1)} %copy-done.5, s32[]{:T(128)S(6)} %select_n.38), kind=kOutput, calls=%fused_computation.11 | convolution fusion | flops 4299161600 | bytes 14680068 | tf_op jit(solution)/shard_map/dot_general | solution.py:183
  153.8 29.5 %reduce-scatter.5.cloned.1.call-done = bf16[512,512]{0,1:T(8,128)(2,1)} async-done(((bf16[2048,512]{0,1:T(8,128)(2,1)}), bf16[512,512]{0,1:T(8,128)(2,1)}) %reduce-scatter.5.cloned.1.call-update) | async-done | bytes 524304 | tf_op jit(solution)/shard_map/reduce_scatter | solution.py:182
  183.3 5.5 %all-to-all-start.1 = ((bf16[512,8,64]{0,2,1:T(8,128)(2,1)}), bf16[512,8,64]{0,2,1:T(8,128)(2,1)S(1)}, u32[]{:S(2)}, u32[]{:S(2)}) async-start(bf16[512,8,64]{0,2,1:T(8,128)(2,1)} %bitcast.96), calls=%async_computation.3 | async-start | bytes 1048576 | tf_op jit(solution)/shard_map/all_to_all | solution.py:190
  188.9 14.3 %all-to-all-done.1 = bf16[512,8,64]{0,2,1:T(8,128)(2,1)S(1)} async-done(((bf16[512,8,64]{0,2,1:T(8,128)(2,1)}), bf16[512,8,64]{0,2,1:T(8,128)(2,1)S(1)}, u32[]{:S(2)}, u32[]{:S(2)}) %all-to-all-start.1) | async-done | bytes 524320 | tf_op jit(solution)/shard_map/all_to_all | solution.py:190
  203.2 0.3 convolution_multiply_fusion.1
  203.4 0.4 fusion.70
  203.8 6.0 %all-reduce = (f32[128]{0:T(128)S(1)}, f32[128]{0:T(128)S(1)}) all-reduce(f32[128]{0:T(128)S(1)} %get-tuple-element.6, f32[128]{0:T(128)S(1)} %get-tuple-element.5), channel_id=1, replica_groups=mesh['sp'=8,'tp'=4] {'tp'}, use_global_device_ids=true, to_apply=%region_16.17 | all-reduce | flops 256 | bytes 2048 | tf_op jit(solution)/shard_map/psum | solution.py:57
  209.8 0.8 fusion.53
  (49 shorter events, 0.4 us)
Async XLA Ops:
  6.5 50.0 %copy-start = (bf16[512,2048]{1,0:T(8,128)(2,1)S(1)}, bf16[512,2048]{1,0:T(8,128)(2,1)}, u32[]{:S(2)}) copy-start(bf16[512,2048]{1,0:T(8,128)(2,1)} %param.20) | copy-start | bytes 6291460
  6.5 46.1 %all-gather.2.cloned.1.call-start = ((), (), s32[]{:S(2)}) async-start(), calls=%async_computation.4 | async-start | bytes 1179648 | tf_op jit(solution)/shard_map/all_gather | solution.py:104
  9.7 0.7 copy-start.2
  10.3 68.3 %reduce-scatter.3.cloned.1.call-start = ((), (), s32[]{:S(2)}) async-start(), calls=%async_computation.5 | async-start | bytes 655360 | tf_op jit(solution)/shard_map/reduce_scatter | solution.py:134
  52.6 2.9 %copy-start.1 = (bf16[1024,512]{0,1:T(8,128)(2,1)S(1)}, bf16[1024,512]{0,1:T(8,128)(2,1)}, u32[]{:S(2)}) copy-start(bf16[1024,512]{0,1:T(8,128)(2,1)} %all-gather.2.cloned.1.call-done) | copy-start | bytes 3145732
  55.5 2.4 %copy-start.6 = (s32[128,2]{0,1:T(2,128)S(1)}, s32[128,2]{0,1:T(2,128)}, u32[]{:S(2)}) copy-start(s32[128,2]{0,1:T(2,128)} %param.22) | copy-start | bytes 3076
  55.5 23.2 %copy-start.3 = (bf16[128,512]{1,0:T(8,128)(2,1)S(1)}, bf16[128,512]{1,0:T(8,128)(2,1)}, u32[]{:S(2)}) copy-start(bf16[128,512]{1,0:T(8,128)(2,1)} %param.19) | copy-start | bytes 393220
  55.5 30.0 %copy-start.10 = (f32[512]{0:T(512)S(1)}, f32[512]{0:T(512)}, u32[]{:S(2)}) copy-start(f32[512]{0:T(512)} %param.21) | copy-start | bytes 6148
  57.8 125.5 %reduce-scatter.5.cloned.1.call-start = ((), (), s32[]{:S(2)}) async-start(), calls=%async_computation.6 | async-start | bytes 2621440 | tf_op jit(solution)/shard_map/reduce_scatter | solution.py:182
  106.5 8.6 %collective-permute-start = (bf16[512,512]{1,0:T(8,128)(2,1)S(1)}, bf16[512,512]{1,0:T(8,128)(2,1)S(1)}, u32[]{:S(2)}, u32[]{:S(2)}) collective-permute-start(bf16[512,512]{1,0:T(8,128)(2,1)S(1)} %bitcast.91), channel_id=1, source_target_pairs={{0,1},{1,2},{2,3},{3,0},{4,5},{5,6},{6,7},{7,4},{8,9},{9,10},{10,1... | collective-permute-start | bytes 1572872 | tf_op jit(solution)/shard_map/ppermute | solution.py:174
  115.1 8.7 %collective-permute-start.1 = (bf16[512,512]{1,0:T(8,128)(2,1)S(1)}, bf16[512,512]{1,0:T(8,128)(2,1)}, u32[]{:S(2)}, u32[]{:S(2)}) collective-permute-start(bf16[512,512]{1,0:T(8,128)(2,1)S(1)} %collective-permute-done), channel_id=1, source_target_pairs={{0,1},{1,2},{2,3},{3,0},{4,5},{5,6},{6,7},{7,4},{8,9},{9,10},{10,1... | collective-permute-start | bytes 1572872 | tf_op jit(solution)/shard_map/ppermute | solution.py:174
  123.9 8.9 %collective-permute-start.2 = (bf16[512,512]{1,0:T(8,128)(2,1)}, bf16[512,512]{1,0:T(8,128)(2,1)}, u32[]{:S(2)}, u32[]{:S(2)}) collective-permute-start(bf16[512,512]{1,0:T(8,128)(2,1)} %collective-permute-done.1), channel_id=1, source_target_pairs={{0,1},{1,2},{2,3},{3,0},{4,5},{5,6},{6,7},{7,4},{8,9},{9,10},{10,1... | collective-permute-start | bytes 1572872 | tf_op jit(solution)/shard_map/ppermute | solution.py:174
  123.9 15.6 %copy-start.9 = (bf16[1,2048,1024]{2,1,0:T(8,128)(2,1)S(1)}, bf16[1,2048,1024]{2,1,0:T(8,128)(2,1)}, u32[]{:S(2)}) copy-start(bf16[1,2048,1024]{2,1,0:T(8,128)(2,1)} %param.24) | copy-start | bytes 12582916
  137.6 1.9 copy-start.5
  143.2 45.6 %copy-start.8 = (f32[128,2]{0,1:T(2,128)S(1)}, f32[128,2]{0,1:T(2,128)}, u32[]{:S(2)}) copy-start(f32[128,2]{0,1:T(2,128)} %param.23) | copy-start | bytes 3076
  143.2 60.2 %copy-start.4 = (bf16[512,128]{0,1:T(8,128)(2,1)S(1)}, bf16[512,128]{0,1:T(8,128)(2,1)}, u32[]{:S(2)}) copy-start(bf16[512,128]{0,1:T(8,128)(2,1)} %reduce-scatter.3.cloned.1.call-done) | copy-start | bytes 393220
  153.8 56.0 %copy-start.7 = (f32[512]{0:T(512)S(1)}, f32[512]{0:T(512)}, u32[]{:S(2)}) copy-start(f32[512]{0:T(512)} %param.27) | copy-start | bytes 6148
  183.3 19.8 %all-to-all-start.1 = ((bf16[512,8,64]{0,2,1:T(8,128)(2,1)}), bf16[512,8,64]{0,2,1:T(8,128)(2,1)S(1)}, u32[]{:S(2)}, u32[]{:S(2)}) async-start(bf16[512,8,64]{0,2,1:T(8,128)(2,1)} %bitcast.96), calls=%async_computation.3 | async-start | bytes 1048576 | tf_op jit(solution)/shard_map/all_to_all | solution.py:190
Sparse Core Ops, SparseCore 0:
  10.5 42.1 all-gather.1
  57.9 20.6 reduce-scatter.2
  154.0 29.3 reduce-scatter.4
